TPU v7x, 32 devices: a whole 2x2x4 slice. The times are simulated.
32 devices in a mesh: sp: 8 (over z, y), tp: 4 (over x, core).
Axes of the slice: x: 2, y: 2, z: 4, core: 2. Of those that a mesh axis runs over, the one named last changes fastest.
Arguments:
- queries: bfloat16 [4096, 512], P('sp', 'tp'), may hold values from -6 to 6
- keys: bfloat16 [4096, 512], P('sp', 'tp'), may hold values from -6 to 6
- values: bfloat16 [4096, 1024], P('sp', 'tp'), may hold values from -6 to 6
- input_gate_log: float32 [8, 4096], P('tp', 'sp'), may hold values from -5 to 128
- forget_gate_logits: float32 [8, 4096], P('tp', 'sp'), may hold values from 1 to 16
- extra_decay_log: float32 [8, 4096], P('tp', 'sp'), may hold values from -1 to 0
- output_gate_logits: bfloat16 [4096, 1024], P('sp', 'tp'), may hold values from -6 to 6
- head_norm_scale: float32 [1024], P('tp'), may hold values from 0.1 to 1.9
- layer_residual_input: bfloat16 [4096, 2048], P(('sp', 'tp')), may hold values from -6 to 6
- output_projection_weight: bfloat16 [1024, 2048], replicated, may hold values from -0.1875 to 0.1875
- expert_norm_scale: float32 [2048], replicated, may hold values from 0.1 to 1.9
- routing_expert_index: int32 [4096, 2], P(('sp', 'tp')), may hold values from 0 to 31, all different within a row; in each aligned block of 128 rows (0 to 127, 128 to 255, ...) at most 16 rows name the same one
- routing_expert_weight: float32 [4096, 2], P(('sp', 'tp')), may hold values from 0.2 to 1
- expert_gate_weight: bfloat16 [32, 2048, 1024], P(('sp', 'tp')), may hold values from -0.125 to 0.125
- expert_up_weight: bfloat16 [32, 2048, 1024], P(('sp', 'tp')), may hold values from -0.125 to 0.125
- expert_down_weight: bfloat16 [32, 1024, 2048], P(('sp', 'tp')), may hold values from -0.1875 to 0.1875
Outputs:
- result: bfloat16 [4096, 2048], P(('sp', 'tp'))
Inputs may be any that keep to these rules, and one draw needn't show every extreme that they name: `routing_expert_index`: each row names 2 different experts. Within each aligned block of 128 rows (the rows of one device) no expert is named more than 16 times, a bound that some block reaches in every draw.
All inputs are finite; a program needn't handle non-finite values.
Results may differ from a plain program's by a relative error of at most 0.013.
Values may be sent and summed in bfloat16 or wider, within the bound.
A program may use at most 64 MiB of HBM per device.

v0:
```python
import jax
import jax.numpy as jnp
from jax import lax
from jax.sharding import PartitionSpec as P

TOP = 2
BLOCK = 128


very_low = -1e30
epsilon = 1e-06
highest = lax.Precision.HIGHEST


def carried_in(shard, axis, combine, identity):
    size, here = (lax.axis_size(axis), lax.axis_index(axis))
    everything = jax.tree.map(lambda part: lax.all_gather(part, axis), shard)
    start = jax.tree.map(
        lambda part, zero: jnp.broadcast_to(jnp.asarray(zero, part.dtype), part.shape),
        shard,
        identity,
    )

    def lap(k, before):
        reached = k < here
        new = combine(before, jax.tree.map(lambda part: part[k], everything))
        return jax.tree.map(lambda a, b: jnp.where(reached, a, b), new, before)

    return lax.fori_loop(0, size, lap, start)


def block_step(carried, inputs):
    memory, stabilizer = carried
    query_blk, key_blk, value_blk, input_blk, forget_blk = inputs
    length = query_blk.shape[1]
    within = jnp.cumsum(forget_blk, axis=-1)
    causal = jnp.arange(length)[:, None] >= jnp.arange(length)[None, :]
    log_weight = jnp.where(
        causal, within[:, :, None] - within[:, None, :] + input_blk[:, None, :], very_low
    )
    from_state = within + stabilizer[:, None]
    largest = jnp.maximum(from_state, jnp.max(log_weight, axis=-1))
    intra_weight = jnp.exp(log_weight - largest[:, :, None])
    state_weight = jnp.exp(from_state - largest)
    scores = jnp.einsum("htd,hsd->hts", query_blk, key_blk, precision=highest) * intra_weight
    numerator = jnp.einsum("hts,hsv->htv", scores, value_blk, precision=highest) + state_weight[
        :, :, None
    ] * jnp.einsum("htd,hdv->htv", query_blk, memory, precision=highest)
    block_total = within[:, -1]
    to_end = block_total[:, None] - within + input_blk
    new_stabilizer = jnp.maximum(block_total + stabilizer, jnp.max(to_end, axis=-1))
    retain = jnp.exp(block_total + stabilizer - new_stabilizer)
    state_add = jnp.exp(to_end - new_stabilizer[:, None])
    memory = retain[:, None, None] * memory + jnp.einsum(
        "hsd,hsv->hdv", key_blk * state_add[:, :, None], value_blk, precision=highest
    )
    return ((memory, new_stabilizer), (numerator, largest))


def join_states(earlier, later):
    decay_early, memory_early, stab_early = earlier
    decay_late, memory_late, stab_late = later
    shifted = decay_late + stab_early
    combined = jnp.maximum(shifted, stab_late)
    early_part = jnp.exp(shifted - combined)
    late_part = jnp.exp(stab_late - combined)
    memory = early_part[:, None, None] * memory_early + late_part[:, None, None] * memory_late
    return (decay_early + decay_late, memory, combined)


def shards(
    queries,
    keys,
    values,
    input_gate_log,
    forget_gate_logits,
    extra_decay_log,
    output_gate_logits,
    head_norm_scale,
    layer_residual_input,
    output_projection_weight,
    expert_norm_scale,
    routing_expert_index,
    routing_expert_weight,
    expert_gate_weight,
    expert_up_weight,
    expert_down_weight,
):
    positions = queries.shape[0]
    heads_here = input_gate_log.shape[0]
    key_width = queries.shape[1] // heads_here
    value_width = values.shape[1] // heads_here
    blocks = positions // BLOCK

    def to_blocks(matrix, columns):
        return (
            matrix.astype(jnp.float32)
            .reshape(blocks, BLOCK, heads_here, columns)
            .transpose(0, 2, 1, 3)
        )

    def gate_blocks(matrix):
        return matrix.reshape(heads_here, blocks, BLOCK).transpose(1, 0, 2)

    query_blocks = to_blocks(queries, key_width) * key_width ** (-0.5)
    key_blocks = to_blocks(keys, key_width)
    value_blocks = to_blocks(values, value_width)
    forget_log_value = jax.nn.log_sigmoid(forget_gate_logits) + extra_decay_log
    sequence_inputs = (
        query_blocks,
        key_blocks,
        value_blocks,
        gate_blocks(input_gate_log),
        gate_blocks(forget_log_value),
    )
    device_decay = jnp.sum(forget_log_value, axis=-1)
    through_here = jnp.cumsum(forget_log_value, axis=-1)
    identity = (
        jnp.zeros((heads_here,), jnp.float32),
        jnp.zeros((heads_here, key_width, value_width), jnp.float32),
        jnp.full((heads_here,), very_low, jnp.float32),
    )
    start_state = (
        jnp.zeros((heads_here, key_width, value_width), jnp.float32),
        jnp.full((heads_here,), very_low, jnp.float32),
    )
    local_state, (numerator, largest) = lax.scan(block_step, start_state, sequence_inputs)
    summary = (device_decay,) + local_state
    incoming = carried_in(summary, "sp", join_states, identity)
    from_start = gate_blocks(through_here) + incoming[2][None, :, None]
    combined = jnp.maximum(largest, from_start)
    old_part = jnp.exp(largest - combined)
    new_part = jnp.exp(from_start - combined)
    numerator = old_part[..., None] * numerator + new_part[..., None] * jnp.einsum(
        "bhtd,hdv->bhtv", query_blocks, incoming[1], precision=highest
    )
    cell_out = numerator.transpose(0, 2, 1, 3).reshape(positions, heads_here, value_width)
    scaled = cell_out * lax.rsqrt(jnp.mean(cell_out * cell_out, axis=-1, keepdims=True) + epsilon)
    gated_out = (
        jax.nn.sigmoid(output_gate_logits.astype(jnp.float32)).reshape(
            positions, heads_here, value_width
        )
        * scaled
        * head_norm_scale.reshape(heads_here, value_width)
    )
    mixture = gated_out.reshape(positions, heads_here * value_width).astype(jnp.bfloat16)
    token_mix = lax.all_to_all(mixture, "tp", split_axis=0, concat_axis=1, tiled=True)
    projected = jnp.dot(token_mix, output_projection_weight, preferred_element_type=jnp.float32)
    middle = (layer_residual_input.astype(jnp.float32) + projected).astype(jnp.bfloat16)
    middle_wide = middle.astype(jnp.float32)
    normed = (
        middle_wide
        * lax.rsqrt(jnp.mean(middle_wide * middle_wide, axis=-1, keepdims=True) + epsilon)
        * expert_norm_scale
    ).astype(jnp.bfloat16)
    tok_count = normed.shape[0]
    model_width = normed.shape[1]
    sp_count = lax.axis_size("sp")
    tp_count = lax.axis_size("tp")
    devices = sp_count * tp_count
    local_experts = expert_gate_weight.shape[0]
    experts = local_experts * devices
    slots = max(2, 2 * tok_count * TOP // experts)
    entries = tok_count * TOP
    flat_ids = routing_expert_index.reshape(-1)
    one_hot = (flat_ids[:, None] == jnp.arange(experts, dtype=jnp.int32)[None, :]).astype(
        jnp.bfloat16
    )
    earlier_rows = (jnp.arange(entries)[:, None] > jnp.arange(entries)[None, :]).astype(
        jnp.bfloat16
    )
    seen_before = jnp.dot(earlier_rows, one_hot, preferred_element_type=jnp.float32)
    position_in = jnp.sum(seen_before * one_hot.astype(jnp.float32), axis=1).astype(jnp.int32)
    slot_key = flat_ids * slots + position_in
    matches = slot_key[None, :] == jnp.arange(experts * slots, dtype=jnp.int32)[:, None]
    source_entry = jnp.sum(
        jnp.where(matches, jnp.arange(entries, dtype=jnp.int32)[None, :], 0), axis=1
    )
    filled = jnp.any(matches, axis=1)
    taken_rows = jnp.take(normed, source_entry // TOP, axis=0)
    outgoing = jnp.where(filled[:, None], taken_rows, jnp.zeros_like(taken_rows)).reshape(
        experts, slots, model_width
    )
    arrived = lax.all_to_all(outgoing, ("sp", "tp"), split_axis=0, concat_axis=0, tiled=True)
    grouped = arrived.reshape(devices, local_experts, arrived.shape[1], model_width)
    gate_part = jnp.einsum(
        "sxcd,xdf->sxcf", grouped, expert_gate_weight, preferred_element_type=jnp.float32
    )
    up_part = jnp.einsum(
        "sxcd,xdf->sxcf", grouped, expert_up_weight, preferred_element_type=jnp.float32
    )
    activation = (jax.nn.silu(gate_part) * up_part).astype(jnp.bfloat16)
    produced = jnp.einsum(
        "sxcf,xfd->sxcd", activation, expert_down_weight, preferred_element_type=jnp.float32
    ).astype(jnp.bfloat16)
    returned = lax.all_to_all(
        produced.reshape(arrived.shape), ("sp", "tp"), split_axis=0, concat_axis=0, tiled=True
    )
    picked = (
        jnp.take(returned.reshape(experts * slots, model_width), slot_key, axis=0)
        .astype(jnp.float32)
        .reshape(tok_count, TOP, model_width)
    )
    expert_sum = jnp.sum(picked * routing_expert_weight[:, :, None], axis=1)
    return (middle_wide + expert_sum).astype(jnp.bfloat16)


def solution(mesh):
    in_specs = (
        P("sp", "tp"),
        P("sp", "tp"),
        P("sp", "tp"),
        P("tp", "sp"),
        P("tp", "sp"),
        P("tp", "sp"),
        P("sp", "tp"),
        P("tp"),
        P(("sp", "tp"), None),
        P(),
        P(),
        P(("sp", "tp"), None),
        P(("sp", "tp"), None),
        P(("sp", "tp"), None, None),
        P(("sp", "tp"), None, None),
        P(("sp", "tp"), None, None),
    )
    out_specs = P(("sp", "tp"), None)
    return jax.shard_map(shards, mesh=mesh, in_specs=in_specs, out_specs=out_specs, check_vma=False)
```

profile of v0, /device:TPU:7, one launch (start us, length us, event | category | flops | bytes accessed | tf_op | source)
XLA Modules:
  0.0 220.2 jit_solution(14258062220592285903)
XLA Ops:
  0.1 1.0 convert_multiply_fusion
  1.3 1.0 copy.71
  2.8 14.0 %while.33 = (s32[]{:T(128)}, f32[2,64,128]{2,1,0:T(8,128)S(1)}, f32[2]{0:T(128)S(1)}, f32[4,2,128,128]{2,3,0,1:T(8,128)S(1)}, f32[4,2,128]{2,0,1:T(4,128)S(1)}, ...) while((s32[]{:T(128)}, f32[2,64,128]{2,1,0:T(8,128)S(1)}, ...), condition=%wide.region_4.5_spmd.clone, body=%wide.region_0.4_spmd.clone.sunk | while | flops 126322440 | bytes 2501925 | solution.py:127
  3.3 0.9 fusion.93
  5.3 0.4 fusion.97
  6.8 0.9 fusion.93
  8.8 0.4 fusion.97
  10.3 0.9 fusion.93
  13.8 0.9 fusion.93
  15.8 0.4 fusion.97
  16.8 0.6 dynamic-slice
  18.5 14.4 %all-reduce.2 = (f32[16]{0:T(128)S(1)}, f32[16]{0:T(128)S(1)}) all-reduce(f32[16]{0:T(128)S(1)} %dynamic-update-slice, f32[16]{0:T(128)S(1)} %dynamic-update-slice.1), channel_id=2, replica_groups=mesh['sp'=8,'tp'=4] {'sp'}, use_global_device_ids=true, to_apply=%add | all-reduce | flops 32 | bytes 256
  33.1 25.3 %all-gather.2 = f32[16,64,128]{2,1,0:T(8,128)S(1)} all-gather(f32[2,64,128]{2,1,0:T(8,128)S(1)} %get-tuple-element.187), channel_id=4, replica_groups=mesh['sp'=8,'tp'=4] {'sp'}, dimensions={0}, use_global_device_ids=true | all-gather | bytes 589824 | tf_op jit(solution)/shard_map/all_gather | solution.py:17
  58.4 1.2 while.34
  59.6 0.6 reduce-window.6
  60.6 0.7 multiply_reduce_fusion.2
  61.8 0.6 mul.196
  62.6 0.8 copy.83
  63.4 13.3 %all-to-all-start = ((bf16[4,128,256]{1,2,0:T(8,128)(2,1)}), bf16[4,128,256]{1,2,0:T(8,128)(2,1)S(1)}, u32[]{:S(2)}, u32[]{:S(2)}) async-start(bf16[4,128,256]{1,2,0:T(8,128)(2,1)} %copy.83), calls=%async_computation | async-start | bytes 524288 | tf_op jit(solution)/shard_map/all_to_all | solution.py:147
  77.8 3.1 %all-to-all-done = bf16[4,128,256]{1,2,0:T(8,128)(2,1)S(1)} async-done(((bf16[4,128,256]{1,2,0:T(8,128)(2,1)}), bf16[4,128,256]{1,2,0:T(8,128)(2,1)S(1)}, u32[]{:S(2)}, u32[]{:S(2)}) %all-to-all-start) | async-done | bytes 262176 | tf_op jit(solution)/shard_map/all_to_all | solution.py:147
  80.9 3.0 %multiply_reduce_fusion.1 = (f32[128]{0:T(128)S(1)}, f32[128,2048]{1,0:T(8,128)S(1)}) fusion(bf16[128,1024]{0,1:T(8,128)(2,1)S(1)} %bitcast.218, bf16[1024,2048]{1,0:T(8,128)(2,1)} %param.29, bf16[128,2048]{1,0:T(8,128)(2,1)S(1)} %copy-done), kind=kOutput, calls=%fused_computation.76 | convolution fusion | flops 538443648 | bytes 6029824 | tf_op jit(solution)/shard_map/dot_general | solution.py:148
  84.2 3.3 %gather_fusion = bf16[512,2048]{1,0:T(8,128)(2,1)} fusion(bf16[128,2048]{1,0:T(8,128)(2,1)S(1)} %multiply_convert_fusion, s32[1024]{0:T(1024)S(1)} %pad_clamp_fusion.1), kind=kCustom, calls=%fused_computation | custom fusion | bytes 4196352 | tf_op jit(solution)/shard_map/jit(_take)/gather | solution.py:180
  87.5 1.9 select_select_fusion
  89.4 55.5 %all_to_all.29 = bf16[32,16,2048]{2,1,0:T(8,128)(2,1)S(1)} all-to-all(bf16[32,16,2048]{2,1,0:T(8,128)(2,1)S(1)} %select_select_fusion), channel_id=1, replica_groups=mesh['sp'=8,'tp'=4] {'sp','tp'}, dimensions={0} | all-to-all | bytes 4194304 | tf_op jit(solution)/shard_map/all_to_all | solution.py:184
  145.0 3.7 %fusion.21 = f32[32,16,1024]{2,1,0:T(8,128)} fusion(bf16[32,16,2048]{2,1,0:T(8,128)(2,1)S(1)} %all_to_all.29, bf16[1,2048,1024]{2,1,0:T(8,128)(2,1)S(1)} %copy-done.9), kind=kOutput, calls=%fused_computation.51 | convolution fusion | flops 2147483648 | bytes 8388608 | tf_op jit(solution)/shard_map/sxcd,xdf->sxcf/dot_general | solution.py:186
  148.7 9.9 %fusion.23 = bf16[32,16,2048]{2,1,0:T(8,128)(2,1)} fusion(bf16[1,1024,2048]{2,1,0:T(8,128)(2,1)} %param.35, bf16[32,16,2048]{2,1,0:T(8,128)(2,1)S(1)} %all_to_all.29, bf16[1,2048,1024]{2,1,0:T(8,128)(2,1)} %param.34, f32[32,16,1024]{2,1,0:T(8,128)} %fusion.21), kind=kOutput, calls=%fused_computation.53 | convolution fusion | flops 4299161600 | bytes 14680064 | tf_op jit(solution)/shard_map/sxcf,xfd->sxcd/dot_general | solution.py:193
  158.6 4.5 %all-to-all-start.2 = ((bf16[32,16,2048]{2,1,0:T(8,128)(2,1)}), bf16[32,16,2048]{2,1,0:T(8,128)(2,1)S(1)}, u32[]{:S(2)}, u32[]{:S(2)}) async-start(bf16[32,16,2048]{2,1,0:T(8,128)(2,1)} %fusion.23), calls=%async_computation.2 | async-start | bytes 4194304 | tf_op jit(solution)/shard_map/all_to_all | solution.py:196
  163.9 47.1 %all-to-all-done.2 = bf16[32,16,2048]{2,1,0:T(8,128)(2,1)S(1)} async-done(((bf16[32,16,2048]{2,1,0:T(8,128)(2,1)}), bf16[32,16,2048]{2,1,0:T(8,128)(2,1)S(1)}, u32[]{:S(2)}, u32[]{:S(2)}) %all-to-all-start.2) | async-done | bytes 2097184 | tf_op jit(solution)/shard_map/all_to_all | solution.py:196
  211.0 2.3 %gather_fusion.1 = bf16[256,2048]{1,0:T(8,128)(2,1)} fusion(bf16[512,2048]{1,0:T(8,128)(2,1)S(1)} %bitcast.206, s32[1024]{0:T(1024)S(1)} %pad_clamp_fusion), kind=kCustom, calls=%fused_computation.1 | custom fusion | bytes 2098176 | tf_op jit(solution)/shard_map/jit(_take)/gather | solution.py:200
  213.4 1.7 gather.15
  215.1 4.1 %multiply_reduce_fusion = f32[128,2048]{1,0:T(8,128)S(1)} fusion(bf16[128,2,2048]{2,1,0:T(2,128)(2,1)S(1)} %gather.15, pred[128,2]{1,0:T(8,128)(4,1)S(1)} %copy.86, f32[128,2]{1,0:T(8,128)S(1)} %copy.88), kind=kLoop, calls=%fused_computation.64 | loop fusion | flops 1835008 | bytes 2098432 | tf_op jit(solution)/shard_map/reduce_sum | solution.py:204
  219.2 0.9 add_convert_fusion
  (169 shorter events, 14.1 us)
Async XLA Ops:
  0.0 2.4 %copy-start.1 = (bf16[512,256]{1,0:T(8,128)(2,1)S(1)}, bf16[512,256]{1,0:T(8,128)(2,1)}, u32[]{:S(2)}) copy-start(bf16[512,256]{1,0:T(8,128)(2,1)} %param.22) | copy-start | bytes 786436
  0.0 2.7 %copy-start.6 = (f32[2,512]{1,0:T(2,128)S(1)}, f32[2,512]{1,0:T(2,128)}, u32[]{:S(2)}) copy-start(f32[2,512]{1,0:T(2,128)} %param.24) | copy-start | bytes 12292
  0.0 2.7 %copy-start.5 = (f32[2,512]{1,0:T(2,128)S(1)}, f32[2,512]{1,0:T(2,128)}, u32[]{:S(2)}) copy-start(f32[2,512]{1,0:T(2,128)} %param.25) | copy-start | bytes 12292
  2.8 14.0 %copy-start.10 = (u32[32]{0:T(128)S(1)}, u32[32]{0:T(128)}, u32[]{:S(2)}) copy-start(u32[32]{0:T(128)} %constant.139) | copy-start | bytes 388
  58.4 4.0 %copy-start.2 = (bf16[512,256]{1,0:T(8,128)(2,1)S(1)}, bf16[512,256]{1,0:T(8,128)(2,1)}, u32[]{:S(2)}) copy-start(bf16[512,256]{1,0:T(8,128)(2,1)} %param.26) | copy-start | bytes 786436
  58.4 4.0 %copy-start.8 = (f32[256]{0:T(256)S(1)}, f32[256]{0:T(256)}, u32[]{:S(2)}) copy-start(f32[256]{0:T(256)} %param.27) | copy-start | bytes 3076
  61.5 15.3 %copy-start.3 = (s32[128,2]{0,1:T(2,128)S(1)}, s32[128,2]{0,1:T(2,128)}, u32[]{:S(2)}) copy-start(s32[128,2]{0,1:T(2,128)} %param.31) | copy-start | bytes 3076
  61.8 19.2 %copy-start = (bf16[128,2048]{1,0:T(8,128)(2,1)S(1)}, bf16[128,2048]{1,0:T(8,128)(2,1)}, u32[]{:S(2)}) copy-start(bf16[128,2048]{1,0:T(8,128)(2,1)} %param.28) | copy-start | bytes 1572868
  63.4 17.5 %all-to-all-start = ((bf16[4,128,256]{1,2,0:T(8,128)(2,1)}), bf16[4,128,256]{1,2,0:T(8,128)(2,1)S(1)}, u32[]{:S(2)}, u32[]{:S(2)}) async-start(bf16[4,128,256]{1,2,0:T(8,128)(2,1)} %copy.83), calls=%async_computation | async-start | bytes 524288 | tf_op jit(solution)/shard_map/all_to_all | solution.py:147
  80.9 3.0 %copy-start.4 = (f32[2048]{0:T(1024)S(1)}, f32[2048]{0:T(1024)}, u32[]{:S(2)}) copy-start(f32[2048]{0:T(1024)} %param.30) | copy-start | bytes 24580
  89.4 55.5 %copy-start.9 = (bf16[1,2048,1024]{2,1,0:T(8,128)(2,1)S(1)}, bf16[1,2048,1024]{2,1,0:T(8,128)(2,1)}, u32[]{:S(2)}) copy-start(bf16[1,2048,1024]{2,1,0:T(8,128)(2,1)} %param.33) | copy-start | bytes 12582916
  158.6 5.2 %copy-start.7 = (f32[128,2]{0,1:T(2,128)S(1)}, f32[128,2]{0,1:T(2,128)}, u32[]{:S(2)}) copy-start(f32[128,2]{0,1:T(2,128)} %param.32) | copy-start | bytes 3076
  158.6 52.5 %all-to-all-start.2 = ((bf16[32,16,2048]{2,1,0:T(8,128)(2,1)}), bf16[32,16,2048]{2,1,0:T(8,128)(2,1)S(1)}, u32[]{:S(2)}, u32[]{:S(2)}) async-start(bf16[32,16,2048]{2,1,0:T(8,128)(2,1)} %fusion.23), calls=%async_computation.2 | async-start | bytes 4194304 | tf_op jit(solution)/shard_map/all_to_all | solution.py:196
where the time goes:
time: 222 us; the launch traced here: 220 us
  blocking collectives  95.2 us (43%)
  waiting for transfers between devices  50.3 us (23%)
  matrix products  22.7 us (10%)
  starting transfers between devices  17.9 us (8%)
  other arithmetic  17 us (8%)
  local copies, waits for them, and re-layouts  15.3 us (7%)
    all_to_all x1, blocking collectives, shards(): lax.all_to_all(outgoing, ('sp', 'tp'), split_axis=0, concat_axis=0, tiled...  55.5 us
    all_to_all x1, waiting for transfers between devices, shards(): lax.all_to_all(produced.reshape(arrived.shape), ('sp', 'tp'), split_axis=...  47.1 us
    all_gather x1, blocking collectives, carried_in(): everything = jax.tree.map(lambda part: lax.all_gather(part, axis), shard)  25.3 us
    unnamed x1, blocking collectives  14.4 us
    all_to_all x1, starting transfers between devices, shards(): lax.all_to_all(mixture, 'tp', split_axis=0, concat_axis=1, tiled=True)  13.3 us
    dot_general x1, matrix products, shards(): jnp.einsum('sxcf,xfd->sxcd', activation, expert_down_weight, preferred_el...  9.89 us
    all_to_all x1, starting transfers between devices, shards(): lax.all_to_all(produced.reshape(arrived.shape), ('sp', 'tp'), split_axis=...  4.52 us
  transfers between devices with their start and end apart: 2, of which 2 were waited for; matrix products, arithmetic and copies ran while one was open for 1% of the time, Pallas kernels for 0%

commit v1 on v0

--- a/solution.py
+++ b/solution.py
@@ -1,6 +1,10 @@
+import functools
+
 import jax
 import jax.numpy as jnp
 from jax import lax
+from jax.experimental import pallas as pl
+from jax.experimental.pallas import tpu as pltpu
 from jax.sharding import PartitionSpec as P
 
 TOP = 2
@@ -10,23 +14,87 @@
 very_low = -1e30
 epsilon = 1e-06
 highest = lax.Precision.HIGHEST
-
-
-def carried_in(shard, axis, combine, identity):
-    size, here = (lax.axis_size(axis), lax.axis_index(axis))
-    everything = jax.tree.map(lambda part: lax.all_gather(part, axis), shard)
-    start = jax.tree.map(
-        lambda part, zero: jnp.broadcast_to(jnp.asarray(zero, part.dtype), part.shape),
-        shard,
-        identity,
-    )
-
-    def lap(k, before):
-        reached = k < here
-        new = combine(before, jax.tree.map(lambda part: part[k], everything))
-        return jax.tree.map(lambda a, b: jnp.where(reached, a, b), new, before)
-
-    return lax.fori_loop(0, size, lap, start)
+MESH = pl.DeviceIdType.MESH
+
+
+def join_kernel(n, heads, key_width, memory_ref, scalars_ref, out_memory, out_scalars,
+                got_memory, got_scalars, send_memory, send_scalars, recv_memory, recv_scalars):
+    me = lax.axis_index("sp")
+    barrier = pltpu.get_barrier_semaphore()
+    for k in range(1, n):
+        other = lax.rem(me + k, n)
+        pl.semaphore_signal(barrier, inc=1, device_id={"sp": other}, device_id_type=MESH)
+    pl.semaphore_wait(barrier, n - 1)
+
+    def copies(source, target):
+        kind = dict(device_id={"sp": target}, device_id_type=MESH)
+        return (
+            pltpu.make_async_remote_copy(
+                src_ref=memory_ref, dst_ref=got_memory.at[source],
+                send_sem=send_memory.at[target], recv_sem=recv_memory.at[source], **kind),
+            pltpu.make_async_remote_copy(
+                src_ref=scalars_ref, dst_ref=got_scalars.at[source],
+                send_sem=send_scalars.at[target], recv_sem=recv_scalars.at[source], **kind),
+        )
+
+    for k in range(n - 1, 0, -1):
+        @pl.when(me + k < n)
+        def _(k=k):
+            for copy in copies(me, me + k):
+                copy.start()
+
+    out_memory[...] = jnp.zeros_like(out_memory)
+    out_scalars[...] = jnp.full_like(out_scalars, very_low)
+
+    def lap(j, carry):
+        for copy in copies(j, me):
+            copy.wait_recv()
+        for h in range(heads):
+            decay = got_scalars[j, h : h + 1, :]
+            stab_late = got_scalars[j, heads + h : heads + h + 1, :]
+            shifted = decay + out_scalars[h : h + 1, :]
+            combined = jnp.maximum(shifted, stab_late)
+            rows = slice(h * key_width, (h + 1) * key_width)
+            out_memory[rows, :] = jnp.exp(shifted - combined) * out_memory[rows, :] + jnp.exp(
+                stab_late - combined
+            ) * got_memory[j, rows, :].astype(jnp.float32)
+            out_scalars[h : h + 1, :] = combined
+        return carry
+
+    lax.fori_loop(0, me, lap, 0)
+    for k in range(1, n):
+        @pl.when(me + k < n)
+        def _(k=k):
+            for copy in copies(me, me + k):
+                copy.wait_send()
+
+
+def incoming_state(decay, memory, stabilizer):
+    heads, key_width, value_width = memory.shape
+    n = lax.axis_size("sp")
+    scalar_rows = -(-2 * heads // 8) * 8
+    scalars = jnp.concatenate(
+        [decay, stabilizer, jnp.zeros((scalar_rows - 2 * heads,), jnp.float32)]
+    )
+    scalars = jnp.broadcast_to(scalars[:, None], (scalar_rows, value_width))
+    flat = memory.reshape(heads * key_width, value_width).astype(jnp.bfloat16)
+    vmem = pl.BlockSpec(memory_space=pltpu.VMEM)
+    out_memory, out_scalars = pl.pallas_call(
+        functools.partial(join_kernel, n, heads, key_width),
+        out_shape=(
+            jax.ShapeDtypeStruct(flat.shape, jnp.float32),
+            jax.ShapeDtypeStruct(scalars.shape, jnp.float32),
+        ),
+        in_specs=[vmem, vmem],
+        out_specs=(vmem, vmem),
+        scratch_shapes=[
+            pltpu.VMEM((n,) + flat.shape, jnp.bfloat16),
+            pltpu.VMEM((n,) + scalars.shape, jnp.float32),
+        ]
+        + [pltpu.SemaphoreType.DMA((n,))] * 4,
+        compiler_params=pltpu.CompilerParams(collective_id=0, has_side_effects=True),
+    )(flat, scalars)
+    return out_memory.reshape(memory.shape), out_scalars[:heads, 0]
 
 
 def block_step(carried, inputs):
@@ -55,17 +123,6 @@
         "hsd,hsv->hdv", key_blk * state_add[:, :, None], value_blk, precision=highest
     )
     return ((memory, new_stabilizer), (numerator, largest))
-
-
-def join_states(earlier, later):
-    decay_early, memory_early, stab_early = earlier
-    decay_late, memory_late, stab_late = later
-    shifted = decay_late + stab_early
-    combined = jnp.maximum(shifted, stab_late)
-    early_part = jnp.exp(shifted - combined)
-    late_part = jnp.exp(stab_late - combined)
-    memory = early_part[:, None, None] * memory_early + late_part[:, None, None] * memory_late
-    return (decay_early + decay_late, memory, combined)
 
 
 def shards(
@@ -115,24 +172,18 @@
     )
     device_decay = jnp.sum(forget_log_value, axis=-1)
     through_here = jnp.cumsum(forget_log_value, axis=-1)
-    identity = (
-        jnp.zeros((heads_here,), jnp.float32),
-        jnp.zeros((heads_here, key_width, value_width), jnp.float32),
-        jnp.full((heads_here,), very_low, jnp.float32),
-    )
     start_state = (
         jnp.zeros((heads_here, key_width, value_width), jnp.float32),
         jnp.full((heads_here,), very_low, jnp.float32),
     )
     local_state, (numerator, largest) = lax.scan(block_step, start_state, sequence_inputs)
-    summary = (device_decay,) + local_state
-    incoming = carried_in(summary, "sp", join_states, identity)
-    from_start = gate_blocks(through_here) + incoming[2][None, :, None]
+    earlier_memory, earlier_max = incoming_state(device_decay, *local_state)
+    from_start = gate_blocks(through_here) + earlier_max[None, :, None]
     combined = jnp.maximum(largest, from_start)
     old_part = jnp.exp(largest - combined)
     new_part = jnp.exp(from_start - combined)
     numerator = old_part[..., None] * numerator + new_part[..., None] * jnp.einsum(
-        "bhtd,hdv->bhtv", query_blocks, incoming[1], precision=highest
+        "bhtd,hdv->bhtv", query_blocks, earlier_memory, precision=highest
     )
     cell_out = numerator.transpose(0, 2, 1, 3).reshape(positions, heads_here, value_width)
     scaled = cell_out * lax.rsqrt(jnp.mean(cell_out * cell_out, axis=-1, keepdims=True) + epsilon)
@@ -173,13 +224,13 @@
     position_in = jnp.sum(seen_before * one_hot.astype(jnp.float32), axis=1).astype(jnp.int32)
     slot_key = flat_ids * slots + position_in
     matches = slot_key[None, :] == jnp.arange(experts * slots, dtype=jnp.int32)[:, None]
-    source_entry = jnp.sum(
-        jnp.where(matches, jnp.arange(entries, dtype=jnp.int32)[None, :], 0), axis=1
-    )
-    filled = jnp.any(matches, axis=1)
-    taken_rows = jnp.take(normed, source_entry // TOP, axis=0)
-    outgoing = jnp.where(filled[:, None], taken_rows, jnp.zeros_like(taken_rows)).reshape(
-        experts, slots, model_width
+    pick = jnp.sum(
+        matches.reshape(experts * slots, tok_count, TOP).astype(jnp.float32), axis=2
+    ).astype(jnp.bfloat16)
+    outgoing = (
+        jnp.dot(pick, normed, preferred_element_type=jnp.float32)
+        .astype(jnp.bfloat16)
+        .reshape(experts, slots, model_width)
     )
     arrived = lax.all_to_all(outgoing, ("sp", "tp"), split_axis=0, concat_axis=0, tiled=True)
     grouped = arrived.reshape(devices, local_experts, arrived.shape[1], model_width)
@@ -196,12 +247,21 @@
     returned = lax.all_to_all(
         produced.reshape(arrived.shape), ("sp", "tp"), split_axis=0, concat_axis=0, tiled=True
     )
-    picked = (
-        jnp.take(returned.reshape(experts * slots, model_width), slot_key, axis=0)
-        .astype(jnp.float32)
-        .reshape(tok_count, TOP, model_width)
-    )
-    expert_sum = jnp.sum(picked * routing_expert_weight[:, :, None], axis=1)
+    returned = returned.reshape(experts * slots, model_width)
+    weight_high = lax.reduce_precision(routing_expert_weight, 8, 7)
+    slot_pairs = slot_key.reshape(tok_count, TOP, 1)
+    slot_range = jnp.arange(experts * slots, dtype=jnp.int32)
+
+    def spread(weights):
+        return jnp.sum(
+            jnp.where(slot_pairs == slot_range, weights[:, :, None], 0.0), axis=1
+        ).astype(jnp.bfloat16)
+
+    expert_sum = jnp.dot(
+        spread(weight_high), returned, preferred_element_type=jnp.float32
+    ) + jnp.dot(
+        spread(routing_expert_weight - weight_high), returned, preferred_element_type=jnp.float32
+    )
     return (middle_wide + expert_sum).astype(jnp.bfloat16)
 
 

time: 222 us -> 171 us (0.77)
  blocking collectives: 95.2 us -> 55 us
  Pallas kernels: 0 us -> 9.2 us
  starting transfers between devices: 17.9 us -> 9.61 us
  local copies, waits for them, and re-layouts: 15.3 us -> 7.49 us
  other arithmetic: 17 us -> 9.56 us
  matrix products: 22.7 us -> 26.1 us
    all_gather x1 -> x0, blocking collectives: 25.3 us -> none  [carried_in(): everything = jax.tree.map(lambda part: lax.all_gather(part, axis), shard)]
    unnamed x1 -> x0, blocking collectives: 14.4 us -> none
    pallas_call x0 -> x1, Pallas kernels: none -> 9.2 us  [incoming_state(): pl.pallas_call(functools.partial(join_kernel, n, heads, key_width), out_s...]
    all_to_all x1, starting transfers between devices: 13.3 us -> 5 us  [shards(): lax.all_to_all(mixture, 'tp', split_axis=0, concat_axis=1, tiled=True)]
    gather x3 -> x0, local copies, waits for them, and re-layouts: 7.44 us -> none  [the longest x2 4.09 us: shards(): jnp.take(returned.reshape(experts * slots, model_width), slot_key, axis=0)]
    reduce_sum x2, other arithmetic: 4.22 us -> 0.26 us  [the longest x1 0.17 us: spread(): jnp.sum(jnp.where(slot_pairs == slot_range, weights[:, :, None], 0.0), ax...]
    dot_general x1 -> x4, matrix products: 0.72 us -> 4.08 us  [the longest x1 1.55 us: shards(): jnp.einsum('bhtd,hdv->bhtv', query_blocks, earlier_memory, precision=high...]
    select_n x19 -> x0, other arithmetic: 2.75 us -> none  [the longest x1 1.91 us: shards(): jnp.where(filled[:, None], taken_rows, jnp.zeros_like(taken_rows))]
where the time goes in v1:
time: 171 us; the launch traced here: 169 us
  blocking collectives  55 us (32%)
  waiting for transfers between devices  51.1 us (30%)
  matrix products  26.1 us (15%)
  starting transfers between devices  9.61 us (6%)
  other arithmetic  9.56 us (6%)
  Pallas kernels  9.2 us (5%)
  local copies, waits for them, and re-layouts  7.49 us (4%)
    all_to_all x1, blocking collectives, shards(): lax.all_to_all(outgoing, ('sp', 'tp'), split_axis=0, concat_axis=0, tiled...  55 us
    all_to_all x1, waiting for transfers between devices, shards(): lax.all_to_all(produced.reshape(arrived.shape), ('sp', 'tp'), split_axis=...  47.7 us
    dot_general x1, matrix products, shards(): jnp.einsum('sxcf,xfd->sxcd', activation, expert_down_weight, preferred_el...  9.9 us
    pallas_call x1, Pallas kernels, incoming_state(): pl.pallas_call(functools.partial(join_kernel, n, heads, key_width), out_s...  9.2 us
    all_to_all x1, starting transfers between devices, shards(): lax.all_to_all(mixture, 'tp', split_axis=0, concat_axis=1, tiled=True)  5 us
    all_to_all x1, starting transfers between devices, shards(): lax.all_to_all(produced.reshape(arrived.shape), ('sp', 'tp'), split_axis=...  4.61 us
    dot_general x1, matrix products, shards(): jnp.einsum('sxcd,xdf->sxcf', grouped, expert_gate_weight, preferred_eleme...  3.75 us
    reduce_max x4, other arithmetic, block_step(): jnp.max(to_end, axis=-1)  3.45 us
  transfers between devices with their start and end apart: 2, of which 2 were waited for; matrix products, arithmetic and copies ran while one was open for 1% of the time, Pallas kernels for 0%

profile of v1, /device:TPU:7, one launch (start us, length us, event | category | flops | bytes accessed | tf_op | source)
XLA Modules:
  0.0 168.8 jit_solution(14177455320679655002)
XLA Ops:
  0.0 1.0 convert_multiply_fusion
  1.2 1.0 copy.79
  2.8 14.0 %while.17 = (s32[]{:T(128)}, f32[2,64,128]{2,1,0:T(8,128)S(1)}, f32[2]{0:T(128)S(1)}, f32[4,2,128,128]{2,3,0,1:T(8,128)S(1)}, f32[4,2,128]{2,0,1:T(4,128)S(1)}, ...) while((s32[]{:T(128)}, f32[2,64,128]{2,1,0:T(8,128)S(1)}, ...), condition=%wide.region_4.5_spmd.clone, body=%wide.region_0.4_spmd.clone.sunk | while | flops 126322440 | bytes 2501925 | solution.py:179
  3.3 0.9 fusion.98
  4.6 0.4 convolution_multiply_fusion.4
  5.3 0.4 fusion.102
  6.8 0.9 fusion.98
  8.1 0.4 convolution_multiply_fusion.4
  8.8 0.4 fusion.102
  10.3 0.9 fusion.98
  12.3 0.4 fusion.102
  13.8 0.9 fusion.98
  15.8 0.4 fusion.102
  16.8 0.6 convert_element_type.77
  17.5 0.7 broadcast_in_dim.50.scalars_ref
  18.1 9.2 %shard_map.154 = (f32[128,128]{1,0:T(8,128)}, f32[8,128]{1,0:T(8,128)}) custom-call(bf16[128,128]{1,0:T(8,128)(2,1)} %bitcast.195, f32[8,128]{1,0:T(8,128)} %broadcast_in_dim.50.scalars_ref), custom_call_target="tpu_custom_call" | custom-call | tf_op jit(solution)/shard_map/pallas_call | solution.py:82
  27.3 0.8 slice_reduce_fusion.2
  28.1 0.6 reduce-window.6
  29.2 1.6 multiply_reduce_fusion.1
  31.2 0.6 mul.133
  32.0 0.8 copy.91
  32.8 5.0 %all-to-all-start = ((bf16[4,128,256]{1,2,0:T(8,128)(2,1)}), bf16[4,128,256]{1,2,0:T(8,128)(2,1)S(1)}, u32[]{:S(2)}, u32[]{:S(2)}) async-start(bf16[4,128,256]{1,2,0:T(8,128)(2,1)} %copy.91), calls=%async_computation | async-start | bytes 524288 | tf_op jit(solution)/shard_map/all_to_all | solution.py:198
  38.6 3.4 %all-to-all-done = bf16[4,128,256]{1,2,0:T(8,128)(2,1)S(1)} async-done(((bf16[4,128,256]{1,2,0:T(8,128)(2,1)}), bf16[4,128,256]{1,2,0:T(8,128)(2,1)S(1)}, u32[]{:S(2)}, u32[]{:S(2)}) %all-to-all-start) | async-done | bytes 262176 | tf_op jit(solution)/shard_map/all_to_all | solution.py:198
  42.0 3.0 %multiply_reduce_fusion = (f32[128]{0:T(128)S(1)}, f32[128,2048]{1,0:T(8,128)S(1)}) fusion(bf16[128,1024]{0,1:T(8,128)(2,1)S(1)} %bitcast.192, bf16[1024,2048]{1,0:T(8,128)(2,1)} %param.27, bf16[128,2048]{1,0:T(8,128)(2,1)S(1)} %copy-done), kind=kOutput, calls=%fused_computation.62 | convolution fusion | flops 538443648 | bytes 6029824 | tf_op jit(solution)/shard_map/dot_general | solution.py:199
  45.1 0.8 convolution_convert_fusion
  45.8 55.0 %all_to_all.29 = bf16[32,16,2048]{2,1,0:T(8,128)(2,1)S(1)} all-to-all(bf16[32,16,2048]{2,1,0:T(8,128)(2,1)S(1)} %bitcast.182), channel_id=1, replica_groups=mesh['sp'=8,'tp'=4] {'sp','tp'}, dimensions={0} | all-to-all | bytes 4194304 | tf_op jit(solution)/shard_map/all_to_all | solution.py:235
  100.8 3.7 %fusion.16 = f32[32,16,1024]{2,1,0:T(8,128)} fusion(bf16[32,16,2048]{2,1,0:T(8,128)(2,1)S(1)} %all_to_all.29, bf16[1,2048,1024]{2,1,0:T(8,128)(2,1)S(1)} %copy-done.9), kind=kOutput, calls=%fused_computation.37 | convolution fusion | flops 2147483648 | bytes 8388608 | tf_op jit(solution)/shard_map/sxcd,xdf->sxcf/dot_general | solution.py:237
  104.6 9.9 %fusion.18 = bf16[32,16,2048]{2,1,0:T(8,128)(2,1)} fusion(bf16[1,1024,2048]{2,1,0:T(8,128)(2,1)} %param.33, bf16[32,16,2048]{2,1,0:T(8,128)(2,1)S(1)} %all_to_all.29, bf16[1,2048,1024]{2,1,0:T(8,128)(2,1)} %param.32, f32[32,16,1024]{2,1,0:T(8,128)} %fusion.16), kind=kOutput, calls=%fused_computation.39 | convolution fusion | flops 4299161600 | bytes 14680064 | tf_op jit(solution)/shard_map/sxcf,xfd->sxcd/dot_general | solution.py:244
  114.5 4.6 %all-to-all-start.2 = ((bf16[32,16,2048]{2,1,0:T(8,128)(2,1)}), bf16[32,16,2048]{2,1,0:T(8,128)(2,1)S(1)}, u32[]{:S(2)}, u32[]{:S(2)}) async-start(bf16[32,16,2048]{2,1,0:T(8,128)(2,1)} %fusion.18), calls=%async_computation.2 | async-start | bytes 4194304 | tf_op jit(solution)/shard_map/all_to_all | solution.py:247
  119.3 47.7 %all-to-all-done.2 = bf16[32,16,2048]{2,1,0:T(8,128)(2,1)S(1)} async-done(((bf16[32,16,2048]{2,1,0:T(8,128)(2,1)}), bf16[32,16,2048]{2,1,0:T(8,128)(2,1)S(1)}, u32[]{:S(2)}, u32[]{:S(2)}) %all-to-all-start.2) | async-done | bytes 2097184 | tf_op jit(solution)/shard_map/all_to_all | solution.py:247
  167.0 0.4 fusion.64
  167.5 1.3 fusion.24
  (121 shorter events, 10.5 us)
Async XLA Ops:
  0.0 2.4 %copy-start.1 = (bf16[512,256]{1,0:T(8,128)(2,1)S(1)}, bf16[512,256]{1,0:T(8,128)(2,1)}, u32[]{:S(2)}) copy-start(bf16[512,256]{1,0:T(8,128)(2,1)} %param.20) | copy-start | bytes 786436
  0.0 2.6 %copy-start.6 = (f32[2,512]{1,0:T(2,128)S(1)}, f32[2,512]{1,0:T(2,128)}, u32[]{:S(2)}) copy-start(f32[2,512]{1,0:T(2,128)} %param.22) | copy-start | bytes 12292
  0.0 2.6 %copy-start.5 = (f32[2,512]{1,0:T(2,128)S(1)}, f32[2,512]{1,0:T(2,128)}, u32[]{:S(2)}) copy-start(f32[2,512]{1,0:T(2,128)} %param.23) | copy-start | bytes 12292
  16.7 15.1 %copy-start.2 = (bf16[512,256]{1,0:T(8,128)(2,1)S(1)}, bf16[512,256]{1,0:T(8,128)(2,1)}, u32[]{:S(2)}) copy-start(bf16[512,256]{1,0:T(8,128)(2,1)} %param.24) | copy-start | bytes 786436
  16.8 15.1 %copy-start.8 = (f32[256]{0:T(256)S(1)}, f32[256]{0:T(256)}, u32[]{:S(2)}) copy-start(f32[256]{0:T(256)} %param.25) | copy-start | bytes 3076
  30.9 6.9 %copy-start.4 = (s32[128,2]{0,1:T(2,128)S(1)}, s32[128,2]{0,1:T(2,128)}, u32[]{:S(2)}) copy-start(s32[128,2]{0,1:T(2,128)} %param.29) | copy-start | bytes 3076
  31.2 10.8 %copy-start = (bf16[128,2048]{1,0:T(8,128)(2,1)S(1)}, bf16[128,2048]{1,0:T(8,128)(2,1)}, u32[]{:S(2)}) copy-start(bf16[128,2048]{1,0:T(8,128)(2,1)} %param.26) | copy-start | bytes 1572868
  32.8 9.2 %all-to-all-start = ((bf16[4,128,256]{1,2,0:T(8,128)(2,1)}), bf16[4,128,256]{1,2,0:T(8,128)(2,1)S(1)}, u32[]{:S(2)}, u32[]{:S(2)}) async-start(bf16[4,128,256]{1,2,0:T(8,128)(2,1)} %copy.91), calls=%async_computation | async-start | bytes 524288 | tf_op jit(solution)/shard_map/all_to_all | solution.py:198
  42.0 3.0 %copy-start.3 = (f32[2048]{0:T(1024)S(1)}, f32[2048]{0:T(1024)}, u32[]{:S(2)}) copy-start(f32[2048]{0:T(1024)} %param.28) | copy-start | bytes 24580
  45.8 55.0 %copy-start.9 = (bf16[1,2048,1024]{2,1,0:T(8,128)(2,1)S(1)}, bf16[1,2048,1024]{2,1,0:T(8,128)(2,1)}, u32[]{:S(2)}) copy-start(bf16[1,2048,1024]{2,1,0:T(8,128)(2,1)} %param.31) | copy-start | bytes 12582916
  114.5 4.6 %copy-start.7 = (f32[128,2]{0,1:T(2,128)S(1)}, f32[128,2]{0,1:T(2,128)}, u32[]{:S(2)}) copy-start(f32[128,2]{0,1:T(2,128)} %param.30) | copy-start | bytes 3076
  114.5 52.5 %all-to-all-start.2 = ((bf16[32,16,2048]{2,1,0:T(8,128)(2,1)}), bf16[32,16,2048]{2,1,0:T(8,128)(2,1)S(1)}, u32[]{:S(2)}, u32[]{:S(2)}) async-start(bf16[32,16,2048]{2,1,0:T(8,128)(2,1)} %fusion.18), calls=%async_computation.2 | async-start | bytes 4194304 | tf_op jit(solution)/shard_map/all_to_all | solution.py:247

commit v2 on v1

--- a/solution.py
+++ b/solution.py
@@ -97,32 +97,198 @@
     return out_memory.reshape(memory.shape), out_scalars[:heads, 0]
 
 
-def block_step(carried, inputs):
-    memory, stabilizer = carried
-    query_blk, key_blk, value_blk, input_blk, forget_blk = inputs
-    length = query_blk.shape[1]
+def all_blocks(query_blk, key_blk, value_blk, input_blk, forget_blk):
+    blocks, heads, length = forget_blk.shape
     within = jnp.cumsum(forget_blk, axis=-1)
     causal = jnp.arange(length)[:, None] >= jnp.arange(length)[None, :]
     log_weight = jnp.where(
-        causal, within[:, :, None] - within[:, None, :] + input_blk[:, None, :], very_low
-    )
-    from_state = within + stabilizer[:, None]
-    largest = jnp.maximum(from_state, jnp.max(log_weight, axis=-1))
-    intra_weight = jnp.exp(log_weight - largest[:, :, None])
-    state_weight = jnp.exp(from_state - largest)
-    scores = jnp.einsum("htd,hsd->hts", query_blk, key_blk, precision=highest) * intra_weight
-    numerator = jnp.einsum("hts,hsv->htv", scores, value_blk, precision=highest) + state_weight[
-        :, :, None
-    ] * jnp.einsum("htd,hdv->htv", query_blk, memory, precision=highest)
-    block_total = within[:, -1]
-    to_end = block_total[:, None] - within + input_blk
-    new_stabilizer = jnp.maximum(block_total + stabilizer, jnp.max(to_end, axis=-1))
-    retain = jnp.exp(block_total + stabilizer - new_stabilizer)
-    state_add = jnp.exp(to_end - new_stabilizer[:, None])
-    memory = retain[:, None, None] * memory + jnp.einsum(
-        "hsd,hsv->hdv", key_blk * state_add[:, :, None], value_blk, precision=highest
-    )
-    return ((memory, new_stabilizer), (numerator, largest))
+        causal, within[..., :, None] - within[..., None, :] + input_blk[..., None, :], very_low
+    )
+    largest = jnp.max(log_weight, axis=-1)
+    intra_weight = jnp.exp(log_weight - largest[..., None])
+    scores = jnp.einsum("bhtd,bhsd->bhts", query_blk, key_blk, precision=highest) * intra_weight
+    numerator = jnp.einsum("bhts,bhsv->bhtv", scores, value_blk, precision=highest)
+    block_total = within[..., -1]
+    to_end = block_total[..., None] - within + input_blk
+    block_max = jnp.max(to_end, axis=-1)
+    state_add = jnp.exp(to_end - block_max[..., None])
+    block_memory = jnp.einsum(
+        "bhsd,bhsv->bhdv", key_blk * state_add[..., None], value_blk, precision=highest
+    )
+    before = [jnp.zeros((heads,), jnp.float32)]
+    memories = [jnp.zeros(block_memory.shape[1:], jnp.float32)]
+    maxima = [jnp.full((heads,), very_low, jnp.float32)]
+    for b in range(blocks):
+        shifted = maxima[b] + block_total[b]
+        combined = jnp.maximum(shifted, block_max[b])
+        memories.append(
+            jnp.exp(shifted - combined)[:, None, None] * memories[b]
+            + jnp.exp(block_max[b] - combined)[:, None, None] * block_memory[b]
+        )
+        maxima.append(combined)
+        before.append(before[b] + block_total[b])
+    return (numerator, largest, within), (before, memories, maxima)
+
+
+def expert_kernel(peers, count, members, tile,
+                  sent_ref, gate_ref, up_ref, down_ref, high_ref, low_ref, middle_ref, out_ref,
+                  arrived, produced, returned, activation, gate_w, up_w, down_w,
+                  send_there, recv_there, send_back, recv_back, weight_sems):
+    sp = lax.axis_index("sp")
+    me = sp * peers + lax.axis_index("tp")
+    groups = count // members
+    own_group = me // members
+    slots, width = sent_ref.shape[1:]
+    hidden = gate_w.shape[1]
+
+    def place(device):
+        return dict(
+            device_id={"sp": device // peers, "tp": lax.rem(device, peers)}, device_id_type=MESH
+        )
+
+    weight_copies = [
+        pltpu.make_async_copy(source.at[0], target, weight_sems.at[k])
+        for k, (source, target) in enumerate(
+            ((gate_ref, gate_w), (up_ref, up_w), (down_ref, down_w))
+        )
+    ]
+    for copy in weight_copies:
+        copy.start()
+
+    def there(source, target):
+        return pltpu.make_async_remote_copy(
+            src_ref=sent_ref.at[target], dst_ref=arrived.at[source],
+            send_sem=send_there.at[target], recv_sem=recv_there.at[source], **place(target))
+
+    def back(source, target):
+        return pltpu.make_async_remote_copy(
+            src_ref=produced.at[target], dst_ref=returned.at[source],
+            send_sem=send_back.at[target], recv_sem=recv_back.at[source], **place(target))
+
+    barrier = pltpu.get_barrier_semaphore()
+
+    def greet(k, carry):
+        pl.semaphore_signal(barrier, inc=1, **place(lax.rem(me + k, count)))
+        return carry
+
+    lax.fori_loop(1, count, greet, 0)
+    pl.semaphore_wait(barrier, count - 1)
+
+    def group_of(step):
+        return lax.rem(own_group + lax.rem(step, 2) * (groups // 2) + step // 2, groups)
+
+    def dispatch(index, carry):
+        target = group_of(lax.rem(index // members + 1, groups)) * members + lax.rem(index, members)
+
+        @pl.when(target != me)
+        def _():
+            there(me, target).start()
+
+        return carry
+
+    lax.fori_loop(0, count, dispatch, 0)
+    arrived[me] = sent_ref[me]
+    for copy in weight_copies:
+        copy.wait()
+
+    def one_group(step, carry):
+        first = group_of(step) * members
+
+        def receive(j, carry):
+            @pl.when(first + j != me)
+            def _():
+                there(first + j, me).wait_recv()
+
+            return carry
+
+        lax.fori_loop(0, members, receive, 0)
+
+        def hidden_tile(t, carry):
+            columns = pl.ds(pl.multiple_of(t * tile, tile), tile)
+            rows = arrived[pl.ds(first, members)].reshape(members * slots, width)
+            gate_part = jnp.dot(rows, gate_w[:, columns], preferred_element_type=jnp.float32)
+            up_part = jnp.dot(rows, up_w[:, columns], preferred_element_type=jnp.float32)
+            activation[:, columns] = (jax.nn.silu(gate_part) * up_part).astype(jnp.bfloat16)
+            return carry
+
+        lax.fori_loop(0, hidden // tile, hidden_tile, 0)
+
+        def width_tile(t, carry):
+            columns = pl.ds(pl.multiple_of(t * tile, tile), tile)
+            part = jnp.dot(
+                activation[...], down_w[:, columns], preferred_element_type=jnp.float32
+            ).astype(jnp.bfloat16)
+            produced[pl.ds(first, members), :, columns] = part.reshape(members, slots, tile)
+            return carry
+
+        lax.fori_loop(0, width // tile, width_tile, 0)
+
+        def give_back(j, carry):
+            @pl.when(first + j != me)
+            def _():
+                back(me, first + j).start()
+
+            return carry
+
+        lax.fori_loop(0, members, give_back, 0)
+        return carry
+
+    lax.fori_loop(0, groups, one_group, 0)
+    returned[me] = produced[me]
+
+    def collect(k, carry):
+        back(lax.rem(me + k, count), me).wait_recv()
+        return carry
+
+    lax.fori_loop(1, count, collect, 0)
+
+    def combine_tile(t, carry):
+        columns = pl.ds(pl.multiple_of(t * tile, tile), tile)
+        rows = returned[:, :, columns].reshape(count * slots, tile)
+        total = jnp.dot(high_ref[...], rows, preferred_element_type=jnp.float32) + jnp.dot(
+            low_ref[...], rows, preferred_element_type=jnp.float32
+        )
+        out_ref[:, columns] = (middle_ref[:, columns].astype(jnp.float32) + total).astype(
+            jnp.bfloat16
+        )
+        return carry
+
+    lax.fori_loop(0, width // tile, combine_tile, 0)
+
+    def finish(k, carry):
+        target = lax.rem(me + k, count)
+        there(me, target).wait_send()
+        back(me, target).wait_send()
+        return carry
+
+    lax.fori_loop(1, count, finish, 0)
+
+
+def expert_call(sent, gate, up, down, high, low, middle):
+    count, slots, width = sent.shape
+    hidden = gate.shape[2]
+    peers = lax.axis_size("tp")
+    vmem = pl.BlockSpec(memory_space=pltpu.VMEM)
+    anywhere = pl.BlockSpec(memory_space=pl.ANY)
+    members = count // 4
+    return pl.pallas_call(
+        functools.partial(expert_kernel, peers, count, members, 256),
+        out_shape=jax.ShapeDtypeStruct(middle.shape, jnp.bfloat16),
+        in_specs=[vmem, anywhere, anywhere, anywhere, vmem, vmem, vmem],
+        out_specs=vmem,
+        scratch_shapes=[
+            pltpu.VMEM(sent.shape, jnp.bfloat16),
+            pltpu.VMEM(sent.shape, jnp.bfloat16),
+            pltpu.VMEM(sent.shape, jnp.bfloat16),
+            pltpu.VMEM((members * slots, hidden), jnp.bfloat16),
+            pltpu.VMEM((width, hidden), jnp.bfloat16),
+            pltpu.VMEM((width, hidden), jnp.bfloat16),
+            pltpu.VMEM((hidden, width), jnp.bfloat16),
+        ]
+        + [pltpu.SemaphoreType.DMA((count,))] * 4
+        + [pltpu.SemaphoreType.DMA((3,))],
+        compiler_params=pltpu.CompilerParams(collective_id=1, has_side_effects=True),
+    )(sent, gate, up, down, high, low, middle)
 
 
 def shards(
@@ -170,20 +336,21 @@
         gate_blocks(input_gate_log),
         gate_blocks(forget_log_value),
     )
-    device_decay = jnp.sum(forget_log_value, axis=-1)
-    through_here = jnp.cumsum(forget_log_value, axis=-1)
-    start_state = (
-        jnp.zeros((heads_here, key_width, value_width), jnp.float32),
-        jnp.full((heads_here,), very_low, jnp.float32),
-    )
-    local_state, (numerator, largest) = lax.scan(block_step, start_state, sequence_inputs)
-    earlier_memory, earlier_max = incoming_state(device_decay, *local_state)
-    from_start = gate_blocks(through_here) + earlier_max[None, :, None]
+    (numerator, largest, within), (before, memories, maxima) = all_blocks(*sequence_inputs)
+    earlier_memory, earlier_max = incoming_state(before[-1], memories[-1], maxima[-1])
+    local_max = jnp.stack(maxima[:-1])
+    moved_max = jnp.stack(before[:-1]) + earlier_max[None, :]
+    start_max = jnp.maximum(moved_max, local_max)
+    start_memory = (
+        jnp.exp(moved_max - start_max)[..., None, None] * earlier_memory[None]
+        + jnp.exp(local_max - start_max)[..., None, None] * jnp.stack(memories[:-1])
+    )
+    from_start = within + start_max[..., None]
     combined = jnp.maximum(largest, from_start)
     old_part = jnp.exp(largest - combined)
     new_part = jnp.exp(from_start - combined)
     numerator = old_part[..., None] * numerator + new_part[..., None] * jnp.einsum(
-        "bhtd,hdv->bhtv", query_blocks, earlier_memory, precision=highest
+        "bhtd,bhdv->bhtv", query_blocks, start_memory, precision=highest
     )
     cell_out = numerator.transpose(0, 2, 1, 3).reshape(positions, heads_here, value_width)
     scaled = cell_out * lax.rsqrt(jnp.mean(cell_out * cell_out, axis=-1, keepdims=True) + epsilon)
@@ -232,6 +399,21 @@
         .astype(jnp.bfloat16)
         .reshape(experts, slots, model_width)
     )
+    weight_high = lax.reduce_precision(routing_expert_weight, 8, 7)
+    slot_pairs = slot_key.reshape(tok_count, TOP, 1)
+    slot_range = jnp.arange(experts * slots, dtype=jnp.int32)
+
+    def spread(weights):
+        return jnp.sum(
+            jnp.where(slot_pairs == slot_range, weights[:, :, None], 0.0), axis=1
+        ).astype(jnp.bfloat16)
+
+    high = spread(weight_high)
+    low = spread(routing_expert_weight - weight_high)
+    if local_experts == 1 and slots % 16 == 0 and devices % 4 == 0:
+        return expert_call(
+            outgoing, expert_gate_weight, expert_up_weight, expert_down_weight, high, low, middle
+        )
     arrived = lax.all_to_all(outgoing, ("sp", "tp"), split_axis=0, concat_axis=0, tiled=True)
     grouped = arrived.reshape(devices, local_experts, arrived.shape[1], model_width)
     gate_part = jnp.einsum(
@@ -248,19 +430,8 @@
         produced.reshape(arrived.shape), ("sp", "tp"), split_axis=0, concat_axis=0, tiled=True
     )
     returned = returned.reshape(experts * slots, model_width)
-    weight_high = lax.reduce_precision(routing_expert_weight, 8, 7)
-    slot_pairs = slot_key.reshape(tok_count, TOP, 1)
-    slot_range = jnp.arange(experts * slots, dtype=jnp.int32)
-
-    def spread(weights):
-        return jnp.sum(
-            jnp.where(slot_pairs == slot_range, weights[:, :, None], 0.0), axis=1
-        ).astype(jnp.bfloat16)
-
-    expert_sum = jnp.dot(
-        spread(weight_high), returned, preferred_element_type=jnp.float32
-    ) + jnp.dot(
-        spread(routing_expert_weight - weight_high), returned, preferred_element_type=jnp.float32
+    expert_sum = jnp.dot(high, returned, preferred_element_type=jnp.float32) + jnp.dot(
+        low, returned, preferred_element_type=jnp.float32
     )
     return (middle_wide + expert_sum).astype(jnp.bfloat16)
 

time: 171 us -> 152 us (0.89)
  Pallas kernels: 9.2 us -> 117 us
  blocking collectives: 55 us -> 0 us
  waiting for transfers between devices: 51.1 us -> 2.48 us
  matrix products: 26.1 us -> 9.38 us
  starting transfers between devices: 9.61 us -> 5.01 us
  local copies, waits for them, and re-layouts: 7.49 us -> 9.64 us
  other arithmetic: 9.56 us -> 7.66 us
    pallas_call x0 -> x1, Pallas kernels: none -> 108 us  [expert_call(): pl.pallas_call(functools.partial(expert_kernel, peers, count, members, 25...]
    all_to_all x1 -> x0, blocking collectives: 55 us -> none  [shards(): lax.all_to_all(outgoing, ('sp', 'tp'), split_axis=0, concat_axis=0, tiled...]
    all_to_all x1 -> x0, waiting for transfers between devices: 47.7 us -> none  [shards(): lax.all_to_all(produced.reshape(arrived.shape), ('sp', 'tp'), split_axis=...]
    dot_general x21 -> x4, matrix products: 22.1 us -> 3.99 us  [the longest x1 1.94 us: shards(): jnp.einsum('bhtd,bhdv->bhtv', query_blocks, start_memory, precision=highest)]
    all_to_all x1 -> x0, starting transfers between devices: 4.61 us -> none  [shards(): lax.all_to_all(produced.reshape(arrived.shape), ('sp', 'tp'), split_axis=...]
    reduce_max x8 -> x2, other arithmetic: 4.17 us -> 1.25 us  [the longest x1 0.84 us: all_blocks(): block_max = jnp.max(to_end, axis=-1)]
    unnamed x21 -> x19, local copies, waits for them, and re-layouts: 0.16 us -> 3.05 us
  transfers between devices with their start and end apart: 2 -> 1, of which waited for: 2 -> 1; matrix products, arithmetic and copies ran while one was open for 1% -> 1% of each run, Pallas kernels for 0% -> 0%
where the time goes in v2:
time: 152 us; the launch traced here: 151 us
  Pallas kernels  117 us (77%)
  local copies, waits for them, and re-layouts  9.64 us (6%)
  matrix products  9.38 us (6%)
  other arithmetic  7.66 us (5%)
  starting transfers between devices  5.01 us (3%)
  waiting for transfers between devices  2.48 us (2%)
    pallas_call x1, Pallas kernels, expert_call(): pl.pallas_call(functools.partial(expert_kernel, peers, count, members, 25...  108 us
    pallas_call x1, Pallas kernels, incoming_state(): pl.pallas_call(functools.partial(join_kernel, n, heads, key_width), out_s...  9.2 us
    all_to_all x1, starting transfers between devices, shards(): lax.all_to_all(mixture, 'tp', split_axis=0, concat_axis=1, tiled=True)  5.01 us
    unnamed x19, local copies, waits for them, and re-layouts  3.05 us
  transfers between devices with their start and end apart: 1, of which 1 were waited for; matrix products, arithmetic and copies ran while one was open for 1% of the time, Pallas kernels for 0%

profile of v2, /device:TPU:7, one launch (start us, length us, event | category | flops | bytes accessed | tf_op | source)
XLA Modules:
  0.0 151.5 jit_solution(877607853484950319)
XLA Ops:
  0.0 0.7 fusion.49
  0.7 1.2 reduce_window_sum.11
  2.0 0.2 slice_reduce_fusion.3
  2.5 0.8 fusion.66
  3.4 0.8 subtract_exponential_fusion
  5.4 1.0 copy.109
  6.5 0.9 convert_multiply_fusion.2
  7.7 1.0 reshape.552
  8.7 0.2 copy.123
  8.9 0.6 fusion.23
  9.7 0.8 fusion.36.memory_ref
  10.6 0.7 broadcast_in_dim.29.scalars_ref
  11.2 9.2 %shard_map.154 = (f32[128,128]{1,0:T(8,128)}, f32[8,128]{1,0:T(8,128)}) custom-call(bf16[128,128]{1,0:T(8,128)(2,1)} %fusion.36.memory_ref, f32[8,128]{1,0:T(8,128)} %broadcast_in_dim.29.scalars_ref), custom_call_target="tpu_custom_call" | custom-call | tf_op jit(solution)/shard_map/pallas_call | solution.py:82
  20.4 0.8 slice_reduce_fusion.1
  21.2 0.4 fusion.14
  21.9 0.8 convolution_multiply_fusion
  22.7 0.7 fusion.3
  23.4 1.9 %multiply_reduce_fusion = (f32[4,128,2]{1,2,0:T(2,128)S(1)}, f32[4,128,2,128]{1,3,2,0:T(8,128)S(1)}) fusion(f32[4,128,2,128]{1,3,2,0:T(8,128)S(1)} %fusion.3, f32[1,2,64,128]{3,2,1,0:T(8,128)S(1)} %get-tuple-element.19, f32[1,2,64,128]{3,2,1,0:T(8,128)S(1)} %get-tuple-element.20, f32[1,2,64,128]{3,2,1,0:T(8,128)S(1)} %get-tuple-element.21, ...), kind=kOutput, calls=%fused_computation.25 | convolution fusion | flops 101579776 | bytes 1581136 | tf_op jit(solution)/shard_map/bhtd,bhdv->bhtv/dot_general | solution.py:352
  25.4 0.2 copy.119
  25.5 0.3 copy.118
  25.8 0.6 mul.325
  26.4 0.2 fusion.11
  26.6 0.8 copy.120
  27.4 5.0 %all-to-all-start = ((bf16[4,128,256]{1,2,0:T(8,128)(2,1)}), bf16[4,128,256]{1,2,0:T(8,128)(2,1)S(1)}, u32[]{:S(2)}, u32[]{:S(2)}) async-start(bf16[4,128,256]{1,2,0:T(8,128)(2,1)} %copy.120), calls=%async_computation | async-start | bytes 524288 | tf_op jit(solution)/shard_map/all_to_all | solution.py:365
  32.6 0.1 eq.21
  32.7 0.2 fusion.4
  33.2 0.9 select_reduce_fusion
  34.1 2.5 %all-to-all-done = bf16[4,128,256]{1,2,0:T(8,128)(2,1)S(1)} async-done(((bf16[4,128,256]{1,2,0:T(8,128)(2,1)}), bf16[4,128,256]{1,2,0:T(8,128)(2,1)S(1)}, u32[]{:S(2)}, u32[]{:S(2)}) %all-to-all-start) | async-done | bytes 262176 | tf_op jit(solution)/shard_map/all_to_all | solution.py:365
  36.6 3.0 %fusion.5 = (f32[128]{0:T(128)S(1)}, bf16[128,2048]{1,0:T(8,128)(2,1)S(1)}) fusion(bf16[128,1024]{0,1:T(8,128)(2,1)S(1)} %bitcast.162, bf16[1024,2048]{1,0:T(8,128)(2,1)} %param.25, bf16[128,2048]{1,0:T(8,128)(2,1)S(1)} %copy-done.1), kind=kOutput, calls=%fused_computation.13 | convolution fusion | flops 538443648 | bytes 5505536 | tf_op jit(solution)/shard_map/dot_general | solution.py:366
  39.7 2.2 %convolution_convert_fusion = bf16[512,2048]{1,0:T(8,128)(2,1)} fusion(bf16[128,2048]{1,0:T(8,128)(2,1)S(1)} %get-tuple-element.56.middle_ref, f32[2048]{0:T(1024)S(1)} %copy-done.4, f32[128]{0:T(128)S(1)} %add_rsqrt_fusion, bf16[512,128]{1,0:T(8,128)(2,1)S(1)} %convert_reduce_fusion), kind=kOutput, calls=%fused_computation | convolution fusion | flops 270532608 | bytes 2761216 | tf_op jit(solution)/shard_map/dot_general | solution.py:398
  41.8 107.8 %shard_map.155 = bf16[128,2048]{1,0:T(8,128)(2,1)} custom-call(bf16[32,16,2048]{2,1,0:T(8,128)(2,1)} %bitcast.159, bf16[1,2048,1024]{2,1,0:T(8,128)(2,1)} %gate_ref.1, bf16[1,2048,1024]{2,1,0:T(8,128)(2,1)} %up_ref.1, bf16[1,1024,2048]{2,1,0:T(8,128)(2,1)} %down_ref.1, bf16[128,512]{1,0:T(8,128)(2,1)} %get-tuple-element.16.high_ref, ...), custom_call_target="tpu_custom_call" | custom-call | tf_op jit(solution)/shard_map/pallas_call | solution.py:274
  149.6 1.9 %copy.139 = bf16[128,2048]{1,0:T(8,128)(2,1)} copy(bf16[128,2048]{1,0:T(8,128)(2,1)} %shard_map.155) | data formatting | bytes 1048576
  (61 shorter events, 2.8 us)
Async XLA Ops:
  0.0 21.2 %copy-start.3 = (f32[2,512]{1,0:T(2,128)S(1)}, f32[2,512]{1,0:T(2,128)}, u32[]{:S(2)}) copy-start(f32[2,512]{1,0:T(2,128)} %param.19) | copy-start | bytes 12292
  8.9 17.5 %copy-start.2 = (bf16[512,256]{1,0:T(8,128)(2,1)S(1)}, bf16[512,256]{1,0:T(8,128)(2,1)}, u32[]{:S(2)}) copy-start(bf16[512,256]{1,0:T(8,128)(2,1)} %param.22) | copy-start | bytes 786436
  8.9 17.5 %copy-start.7 = (f32[256]{0:T(256)S(1)}, f32[256]{0:T(256)}, u32[]{:S(2)}) copy-start(f32[256]{0:T(256)} %param.23) | copy-start | bytes 3076
  21.9 10.5 %copy-start.6 = (f32[128,2]{0,1:T(2,128)S(1)}, f32[128,2]{0,1:T(2,128)}, u32[]{:S(2)}) copy-start(f32[128,2]{0,1:T(2,128)} %param.28) | copy-start | bytes 3076
  21.9 10.5 %copy-start.5 = (s32[128,2]{0,1:T(2,128)S(1)}, s32[128,2]{0,1:T(2,128)}, u32[]{:S(2)}) copy-start(s32[128,2]{0,1:T(2,128)} %param.27) | copy-start | bytes 3076
  22.7 13.9 %copy-start.1 = (bf16[128,2048]{1,0:T(8,128)(2,1)S(1)}, bf16[128,2048]{1,0:T(8,128)(2,1)}, u32[]{:S(2)}) copy-start(bf16[128,2048]{1,0:T(8,128)(2,1)} %param.24) | copy-start | bytes 1572868
  26.4 13.3 %copy-start.4 = (f32[2048]{0:T(1024)S(1)}, f32[2048]{0:T(1024)}, u32[]{:S(2)}) copy-start(f32[2048]{0:T(1024)} %param.26) | copy-start | bytes 24580
  27.4 9.2 %all-to-all-start = ((bf16[4,128,256]{1,2,0:T(8,128)(2,1)}), bf16[4,128,256]{1,2,0:T(8,128)(2,1)S(1)}, u32[]{:S(2)}, u32[]{:S(2)}) async-start(bf16[4,128,256]{1,2,0:T(8,128)(2,1)} %copy.120), calls=%async_computation | async-start | bytes 524288 | tf_op jit(solution)/shard_map/all_to_all | solution.py:365
  39.6 2.2 %copy-start = (bf16[128,2048]{1,0:T(8,128)(2,1)}, bf16[128,2048]{1,0:T(8,128)(2,1)S(1)}, u32[]{:S(2)}) copy-start(bf16[128,2048]{1,0:T(8,128)(2,1)S(1)} %get-tuple-element.56.middle_ref) | copy-start | bytes 1572868
